TPU v7x, 512 devices: a whole 4x4x16 slice. The times are simulated.
512 devices in a mesh: fs: 16 (over y, x), tp: 32 (over z, core).
Axes of the slice: x: 4, y: 4, z: 16, core: 2. Of those that a mesh axis runs over, the one named last changes fastest.
Arguments:
- tokens: bfloat16 [4096, 2048], P('fs', 'tp'), may hold values from -60 to 60
- norm_gain: float32 [2048], P('fs'), may hold values from 0.1 to 1.9
- gate_weight: float32 [16, 2048, 4096], P(None, 'fs', 'tp'), may hold values from -0.125 to 0.125
- up_weight: float32 [16, 2048, 4096], P(None, 'fs', 'tp'), may hold values from -0.125 to 0.125
- down_weight: float32 [16, 2048, 4096], P(None, 'fs', 'tp'), may hold values from -0.1875 to 0.1875
- route: int32 [4096, 2], P('fs'), may hold values from 0 to 15, all different within a row; in each aligned block of 256 rows (0 to 255, 256 to 511, ...) at most 64 rows name the same one
- route_weight: float32 [4096, 2], P('fs'), may hold values from 0.2 to 1
Outputs:
- mixed: bfloat16 [4096, 2048], P('fs', 'tp')
- gate_new: bfloat16 [16, 2048, 4096], P('fs', None, 'tp')
- up_new: bfloat16 [16, 2048, 4096], P('fs', None, 'tp')
- down_new: bfloat16 [16, 2048, 4096], P('fs', None, 'tp')
Inputs may be any that keep to these rules, and one draw needn't show every extreme that they name: `route`: the 2 experts of a row differ. In each aligned block of 256 rows (the tokens of one index of fs) no expert is named by more than 64 rows, a bound that some block reaches.
All inputs are finite; a program needn't handle non-finite values.
Results may differ from a plain program's by a relative error of at most 0.024.
Values may be sent and summed in bfloat16 or wider, within the bound.
A program may use at most 64 MiB of HBM per device.

v0:
```python
import jax
import jax.numpy as jnp
from jax import lax
from jax.sharding import Mesh
from jax.sharding import PartitionSpec as P

TP = ("tp_0", "tp_1")


epsilon = 1e-05


def sent_together(arrays, axis, split_dim, concat_dim, along):
    both = jnp.concatenate(arrays, axis=along)
    whole, at, done = (
        lax.all_to_all(both, axis, split_axis=split_dim, concat_axis=concat_dim, tiled=True),
        0,
        [],
    )
    for a in arrays:
        done.append(lax.slice_in_dim(whole, at, at + a.shape[along], axis=along))
        at += a.shape[along]
    return tuple(done)


def sent_to_all(x, axis):
    peers = lax.axis_size(axis)
    return lax.all_to_all(jnp.broadcast_to(x[None], (peers, *x.shape)), axis, 0, 0, tiled=True)


def taken_together(x, axis):
    return sent_to_all(x, axis).sum(axis=0)


def reduced_to_own(pieces, axes, turns):
    shape = [lax.axis_size(a) for a in axes]
    pieces = pieces.reshape(*shape, *pieces.shape[1:])
    pieces = pieces.transpose(*turns, *range(len(axes), pieces.ndim))
    pieces = pieces.reshape(-1, *pieces.shape[len(axes) :])
    for k in turns:
        pieces = lax.psum_scatter(pieces, axes[k], scatter_dimension=0, tiled=True)
    return pieces[0]


def in_blocks(x, dim, peers):
    shape = x.shape
    pieces = x.reshape(*shape[:dim], peers, shape[dim] // peers, *shape[dim + 1 :])
    return jnp.moveaxis(pieces, dim, 0)


def scatter_axes(x, axes, turns, dim):
    peers = lax.axis_size(axes)
    return reduced_to_own(in_blocks(x, dim, peers), axes, turns)


def slot_table(route, block_rows, expert_count):
    pair_ids = route.reshape(-1, block_rows * route.shape[1])
    onehot = (
        pair_ids[:, :, None] == jnp.arange(expert_count, dtype=jnp.int32)[None, None, :]
    ).astype(jnp.int32)
    before = jnp.cumsum(onehot, axis=1) - onehot
    return jnp.sum(before * onehot, axis=2).reshape(route.shape)


def body(tokens, norm_gain, gate_weight, up_weight, down_weight, route, route_weight):
    experts = gate_weight.shape[0]
    tok_rows = tokens.shape[0]
    columns = tokens.shape[1]
    fs_count = lax.axis_size("fs")
    capacity = 4 * tok_rows // fs_count
    gain_col = norm_gain[None, :, None]
    gate_cast = (gate_weight * gain_col).astype(jnp.bfloat16)
    up_cast = (up_weight * gain_col).astype(jnp.bfloat16)
    down_cast = down_weight.astype(jnp.bfloat16)
    gate_new, up_new, down_new = sent_together((gate_cast, up_cast, down_cast), "fs", 0, 1, 2)
    slot_of = slot_table(route, tok_rows, experts)
    target = route * capacity + slot_of
    slot_lanes = jnp.arange(experts * capacity, dtype=jnp.int32)
    slot_hits = target[:, :, None] == slot_lanes[None, None, :]
    token_iota = jnp.arange(tok_rows, dtype=jnp.int32)[:, None, None]
    lane_token = jnp.sum(jnp.where(slot_hits, token_iota + 1, 0), axis=(0, 1)) - 1
    lane_token = jnp.where(lane_token < 0, tok_rows, lane_token)
    combine = jnp.sum(jnp.where(slot_hits, route_weight[:, :, None], 0.0), axis=1)
    tok_float = tokens.astype(jnp.float32)
    square_sum = taken_together(jnp.sum(tok_float * tok_float, axis=1), TP)
    full_width = columns * lax.axis_size(TP)
    normed = (tok_float * lax.rsqrt(square_sum / full_width + epsilon)[:, None]).astype(
        jnp.bfloat16
    )
    padded = jnp.concatenate([normed, jnp.zeros((1, columns), jnp.bfloat16)], axis=0)
    outgoing = padded[lane_token].reshape(experts, capacity, columns)
    arrived = lax.all_to_all(outgoing, "fs", split_axis=0, concat_axis=0, tiled=True).reshape(
        -1, columns
    )
    gate_local = gate_new[0]
    up_local = up_new[0]
    piece_rows = lax.all_gather(arrived, TP, axis=1, tiled=True)
    gate_acc = jnp.dot(piece_rows, gate_local, preferred_element_type=jnp.float32)
    up_acc = jnp.dot(piece_rows, up_local, preferred_element_type=jnp.float32)
    hidden = (jax.nn.silu(gate_acc) * up_acc).astype(jnp.bfloat16)
    down_local = down_new[0]
    summed = scatter_axes(
        lax.dot_general(
            down_local, hidden, (((1,), (1,)), ((), ())), preferred_element_type=jnp.float32
        ).astype(jnp.bfloat16),
        TP,
        (1, 0),
        0,
    ).astype(jnp.float32)
    own_columns = summed.shape[0]
    outgoing_back = summed.astype(jnp.bfloat16).reshape(own_columns, fs_count, capacity)
    returned = lax.all_to_all(outgoing_back, "fs", split_axis=1, concat_axis=1, tiled=True).reshape(
        own_columns, experts * capacity
    )
    mixed = lax.dot_general(
        combine,
        returned.astype(jnp.float32),
        (((1,), (1,)), ((), ())),
        preferred_element_type=jnp.float32,
    )
    return (mixed.astype(jnp.bfloat16), gate_new, up_new, down_new)


def solution(mesh):
    split = Mesh(mesh.devices.reshape(mesh.shape["fs"], 16, 2), ("fs", "tp_0", "tp_1"))
    in_specs = (
        P("fs", TP),
        P("fs"),
        P(None, "fs", TP),
        P(None, "fs", TP),
        P(None, "fs", TP),
        P("fs", None),
        P("fs", None),
    )
    out_specs = (P("fs", TP), P("fs", None, TP), P("fs", None, TP), P("fs", None, TP))
    return jax.shard_map(body, mesh=split, in_specs=in_specs, out_specs=out_specs, check_vma=False)
```

profile of v0, /device:TPU:32, one launch (start us, length us, event | category | flops | bytes accessed | tf_op | source)
XLA Modules:
  0.0 259.3 jit_solution(12488290934281086768)
XLA Ops:
  7.2 0.8 fusion.12
  7.9 0.6 broadcast_in_dim.45
  8.6 15.4 %all-to-all-start.1 = ((f32[32,1,256]{2,1,0:T(1,128)}), f32[32,1,256]{2,1,0:T(1,128)S(1)}, u32[]{:S(2)}, u32[]{:S(2)}) async-start(f32[32,1,256]{2,1,0:T(1,128)} %broadcast_in_dim.45), calls=%async_computation.1 | async-start | bytes 65536 | tf_op jit(solution)/shard_map/all_to_all | solution.py:28
  23.9 0.0 all-gather.2.cloned.1.call-start
  24.0 0.8 copy.71
  24.8 0.1 eq.40
  25.0 1.2 reduce-window.6
  26.2 0.2 slice_reduce_fusion
  26.5 0.1 copy.74
  26.5 0.1 broadcast.115
  26.6 0.1 fusion.14
  26.7 0.1 reshape.194
  26.9 0.1 copy.75
  26.9 0.7 multiply_add_fusion
  27.6 0.3 select_reduce_fusion
  28.0 7.7 %all-to-all-done.1 = f32[32,1,256]{2,1,0:T(1,128)S(1)} async-done(((f32[32,1,256]{2,1,0:T(1,128)}), f32[32,1,256]{2,1,0:T(1,128)S(1)}, u32[]{:S(2)}, u32[]{:S(2)}) %all-to-all-start.1) | async-done | bytes 32800 | tf_op jit(solution)/shard_map/all_to_all | solution.py:28
  35.7 0.1 reduce_sum.48
  35.8 0.8 fusion.13
  36.5 0.1 copy.84
  36.7 3.2 %gather_fusion = bf16[1024,64]{1,0:T(8,128)(2,1)S(1)} fusion(bf16[257,64]{1,0:T(8,128)(2,1)S(1)} %concatenate.7.clone, s32[1024]{0:T(1024)S(1)} %broadcast_clamp_fusion), kind=kCustom, calls=%fused_computation | custom fusion | bytes 266240 | tf_op jit(solution)/shard_map/gather | solution.py:91
  39.9 0.0 copy-start.4
  39.9 0.0 copy-start.5
  39.9 0.0 copy-start.7
  39.9 0.2 reshape.209
  40.2 15.1 %all_to_all.28 = bf16[16,2,2048]{2,1,0:T(2,128)(2,1)} all-to-all(bf16[16,2,2048]{2,1,0:T(2,128)(2,1)S(1)} %reshape.209), channel_id=1, replica_groups=mesh['fs'=16,'tp_0'=16,'tp_1'=2] {'fs'}, dimensions={0} | all-to-all | bytes 262144 | tf_op jit(solution)/shard_map/all_to_all | solution.py:92
  55.2 1.1 reshape.210
  56.4 0.8 copy.82
  57.1 0.0 all-gather.2.cloned.1.call-update
  57.2 0.0 reduce-scatter.3.cloned.1.call-start
  57.2 0.0 copy-done.3
  57.2 0.1 convert_element_type.41
  57.3 0.0 copy-done.4
  57.3 0.0 copy-done.5
  57.3 0.0 copy-done.7
  57.3 0.3 multiply_convert_fusion.1
  57.7 0.2 pad_maximum_fusion
  57.9 24.3 %all_to_all.29 = bf16[16,128,384]{2,1,0:T(8,128)(2,1)S(1)} all-to-all(bf16[16,128,384]{2,1,0:T(8,128)(2,1)S(1)} %pad_maximum_fusion), channel_id=1, replica_groups=mesh['fs'=16,'tp_0'=16,'tp_1'=2] {'fs'}, dimensions={0} | all-to-all | bytes 3145728 | tf_op jit(solution)/shard_map/all_to_all | solution.py:16
  82.3 0.3 fusion.16
  82.6 0.0 copy-start
  82.6 0.0 copy-start.1
  82.6 0.0 copy-start.2
  82.6 37.4 %all-gather.2.cloned.1.call-done = bf16[1024,2048]{0,1:T(8,128)(2,1)} async-done(((bf16[1024,64]{0,1:T(8,128)(2,1)}), bf16[1024,2048]{0,1:T(8,128)(2,1)}) %all-gather.2.cloned.1.call-update) | async-done | bytes 4194320 | tf_op jit(solution)/shard_map/all_gather | solution.py:97
  120.0 3.5 %fusion.3 = f32[1024,128]{1,0:T(8,128)S(1)} fusion(bf16[1024,2048]{0,1:T(8,128)(2,1)} %all-gather.2.cloned.1.call-done, bf16[1,2048,128]{2,1,0:T(8,128)(2,1)S(1)} %get-tuple-element.4), kind=kOutput, calls=%fused_computation.12 | convolution fusion | flops 536870912 | bytes 5242880 | tf_op jit(solution)/shard_map/dot_general | solution.py:98
  123.5 0.0 copy-done
  123.5 0.0 copy-done.1
  123.5 0.0 copy-done.2
  123.5 8.6 %convolution_convert_fusion = bf16[2048,1024]{1,0:T(8,128)(2,1)} fusion(bf16[1024,2048]{0,1:T(8,128)(2,1)} %all-gather.2.cloned.1.call-done, bf16[1,2048,128]{2,1,0:T(8,128)(2,1)S(1)} %get-tuple-element.5, bf16[1,2048,128]{2,1,0:T(8,128)(2,1)S(1)} %get-tuple-element.6, f32[1024,128]{1,0:T(8,128)S(1)} %fusion.3), kind=kOutput, calls=%fused_computation.1 | convolution fusion | flops 1076625408 | bytes 9961472 | tf_op jit(solution)/shard_map/dot_general | solution.py:103
  132.1 4.8 %copy.79 = bf16[16,2,64,1024]{3,2,0,1:T(8,128)(2,1)} copy(bf16[16,2,64,1024]{3,2,1,0:T(8,128)(2,1)} %bitcast.42) | data formatting | bytes 8388608 | tf_op jit(solution)/shard_map/reshape;reshape | solution.py:37
  136.9 0.0 reduce-scatter.3.cloned.1.call-update
  137.0 0.0 copy-start.6
  137.0 0.0 reduce-scatter.5.cloned.1.call-start
  137.0 19.7 %reduce-scatter.3.cloned.1.call-done = bf16[16,64,1024]{2,1,0:T(8,128)(2,1)} async-done(((bf16[32,64,1024]{2,1,0:T(8,128)(2,1)}), bf16[16,64,1024]{2,1,0:T(8,128)(2,1)}) %reduce-scatter.3.cloned.1.call-update) | async-done | bytes 2097168 | tf_op jit(solution)/shard_map/reduce_scatter | solution.py:41
  156.7 0.0 reduce-scatter.5.cloned.1.call-update
  156.7 77.7 %reduce-scatter.5.cloned.1.call-done = bf16[1,64,1024]{2,1,0:T(8,128)(2,1)} async-done(((bf16[16,64,1024]{2,1,0:T(8,128)(2,1)}), bf16[1,64,1024]{2,1,0:T(8,128)(2,1)}) %reduce-scatter.5.cloned.1.call-update) | async-done | bytes 131088 | tf_op jit(solution)/shard_map/reduce_scatter | solution.py:41
  234.4 1.1 reshape.198
  235.5 0.1 copy.86
  235.6 0.9 reshape.211
  236.5 6.8 %all-to-all-start.3 = ((bf16[16,2,2048]{2,1,0:T(2,128)(2,1)}), bf16[16,2,2048]{2,1,0:T(2,128)(2,1)S(1)}, u32[]{:S(2)}, u32[]{:S(2)}) async-start(bf16[16,2,2048]{2,1,0:T(2,128)(2,1)} %reshape.211), calls=%async_computation.5 | async-start | bytes 262144 | tf_op jit(solution)/shard_map/all_to_all | solution.py:112
  243.3 0.3 select_reduce_fusion.1
  243.6 7.7 %all-to-all-done.3 = bf16[16,2,2048]{2,1,0:T(2,128)(2,1)S(1)} async-done(((bf16[16,2,2048]{2,1,0:T(2,128)(2,1)}), bf16[16,2,2048]{2,1,0:T(2,128)(2,1)S(1)}, u32[]{:S(2)}, u32[]{:S(2)}) %all-to-all-start.3) | async-done | bytes 131104 | tf_op jit(solution)/shard_map/all_to_all | solution.py:112
  251.3 0.2 reshape.212
  251.5 0.2 copy.81
  251.7 0.2 reshape.199
  251.9 0.9 fusion.17
  (13 shorter events, 0.1 us)
Async XLA Ops:
  8.6 27.1 %all-to-all-start.1 = ((f32[32,1,256]{2,1,0:T(1,128)}), f32[32,1,256]{2,1,0:T(1,128)S(1)}, u32[]{:S(2)}, u32[]{:S(2)}) async-start(f32[32,1,256]{2,1,0:T(1,128)} %broadcast_in_dim.45), calls=%async_computation.1 | async-start | bytes 65536 | tf_op jit(solution)/shard_map/all_to_all | solution.py:28
  23.9 96.1 %all-gather.2.cloned.1.call-start = ((), (), s32[]{:S(2)}) async-start(), calls=%async_computation.6 | async-start | bytes 4325376 | tf_op jit(solution)/shard_map/all_gather | solution.py:97
  36.5 20.7 %copy-start.3 = (f32[16,128,128]{2,1,0:T(8,128)S(1)}, f32[16,128,128]{2,1,0:T(8,128)}, u32[]{:S(2)}) copy-start(f32[16,128,128]{2,1,0:T(8,128)} %param.11) | copy-start | bytes 3145732
  39.9 17.4 %copy-start.4 = (f32[16,128,128]{2,1,0:T(8,128)S(1)}, f32[16,128,128]{2,1,0:T(8,128)}, u32[]{:S(2)}) copy-start(f32[16,128,128]{2,1,0:T(8,128)} %param.9) | copy-start | bytes 3145732
  39.9 17.4 %copy-start.5 = (f32[16,128,128]{2,1,0:T(8,128)S(1)}, f32[16,128,128]{2,1,0:T(8,128)}, u32[]{:S(2)}) copy-start(f32[16,128,128]{2,1,0:T(8,128)} %param.10) | copy-start | bytes 3145732
  39.9 17.4 %copy-start.7 = (f32[128]{0:T(128)S(1)}, f32[128]{0:T(128)}, u32[]{:S(2)}) copy-start(f32[128]{0:T(128)} %param.8) | copy-start | bytes 1540
  57.2 99.5 %reduce-scatter.3.cloned.1.call-start = ((), (), s32[]{:S(2)}) async-start(), calls=%async_computation.7 | async-start | bytes 6291456 | tf_op jit(solution)/shard_map/reduce_scatter | solution.py:41
  82.6 40.9 %copy-start = (bf16[1,2048,128]{2,1,0:T(8,128)(2,1)}, bf16[1,2048,128]{2,1,0:T(8,128)(2,1)S(1)}, u32[]{:S(2)}) copy-start(bf16[1,2048,128]{2,1,0:T(8,128)(2,1)S(1)} %get-tuple-element.4) | copy-start | bytes 1572868
  82.6 40.9 %copy-start.1 = (bf16[1,2048,128]{2,1,0:T(8,128)(2,1)}, bf16[1,2048,128]{2,1,0:T(8,128)(2,1)S(1)}, u32[]{:S(2)}) copy-start(bf16[1,2048,128]{2,1,0:T(8,128)(2,1)S(1)} %get-tuple-element.5) | copy-start | bytes 1572868
  82.6 40.9 %copy-start.2 = (bf16[1,2048,128]{2,1,0:T(8,128)(2,1)}, bf16[1,2048,128]{2,1,0:T(8,128)(2,1)S(1)}, u32[]{:S(2)}) copy-start(bf16[1,2048,128]{2,1,0:T(8,128)(2,1)S(1)} %get-tuple-element.6) | copy-start | bytes 1572868
  137.0 106.3 %copy-start.6 = (f32[256,2]{0,1:T(2,128)S(1)}, f32[256,2]{0,1:T(2,128)}, u32[]{:S(2)}) copy-start(f32[256,2]{0,1:T(2,128)} %param.13) | copy-start | bytes 6148
  137.0 97.4 %reduce-scatter.5.cloned.1.call-start = ((), (), s32[]{:S(2)}) async-start(), calls=%async_computation.8 | async-start | bytes 2228224 | tf_op jit(solution)/shard_map/reduce_scatter | solution.py:41
  236.5 14.8 %all-to-all-start.3 = ((bf16[16,2,2048]{2,1,0:T(2,128)(2,1)}), bf16[16,2,2048]{2,1,0:T(2,128)(2,1)S(1)}, u32[]{:S(2)}, u32[]{:S(2)}) async-start(bf16[16,2,2048]{2,1,0:T(2,128)(2,1)} %reshape.211), calls=%async_computation.5 | async-start | bytes 262144 | tf_op jit(solution)/shard_map/all_to_all | solution.py:112
Sparse Core Ops, SparseCore 0:
  57.3 62.7 all-gather.1
  137.1 19.5 reduce-scatter.2
  159.5 74.8 reduce-scatter.4
where the time goes:
time: 260 us; the launch traced here: 259 us
  waiting for transfers between devices  150 us (58%)
  blocking collectives  39.4 us (15%)
  starting transfers between devices  22.3 us (9%)
  local copies, waits for them, and re-layouts  15.5 us (6%)
  between operations  14.1 us (5%)
  matrix products  13 us (5%)
  other arithmetic  4.87 us (2%)
    reduce_scatter x2, waiting for transfers between devices, reduced_to_own(): pieces = lax.psum_scatter(pieces, axes[k], scatter_dimension=0, tiled=True)  97.4 us
    all_gather x1, waiting for transfers between devices, body(): piece_rows = lax.all_gather(arrived, TP, axis=1, tiled=True)  37.4 us
    all_to_all x1, blocking collectives, sent_together(): lax.all_to_all(both, axis, split_axis=split_dim, concat_axis=concat_dim,...  24.3 us
    all_to_all x1, starting transfers between devices, sent_to_all(): lax.all_to_all(jnp.broadcast_to(x[None], (peers, *x.shape)), axis, 0, 0,...  15.4 us
    all_to_all x1, blocking collectives, body(): lax.all_to_all(outgoing, 'fs', split_axis=0, concat_axis=0, tiled=True)  15.1 us
    dot_general x1, matrix products, body(): lax.dot_general(down_local, hidden, (((1,), (1,)), ((), ())), preferred_e...  8.59 us
    all_to_all x1, waiting for transfers between devices, sent_to_all(): lax.all_to_all(jnp.broadcast_to(x[None], (peers, *x.shape)), axis, 0, 0,...  7.74 us
    all_to_all x1, waiting for transfers between devices, body(): lax.all_to_all(outgoing_back, 'fs', split_axis=1, concat_axis=1, tiled=True)  7.69 us
  transfers between devices with their start and end apart: 5, of which 5 were waited for; matrix products, arithmetic and copies ran while one was open for 2% of the time, Pallas kernels for 0%

commit v1 on v0

v1 whole, which is shorter than its diff:
```python
import jax
import jax.numpy as jnp
from jax import lax
from jax.experimental import pallas as pl
from jax.experimental.pallas import tpu as pltpu
from jax.sharding import PartitionSpec as P

MESH = pl.DeviceIdType.MESH
EPS = 1e-05
F32 = jnp.float32
BF16 = jnp.bfloat16

FS = 16
NZ = 16
HALF = NZ // 2
QUARTERS = 4


def packed(y, p):
    lane = lax.broadcasted_iota(jnp.int32, (32, 128), 1)
    top = y[0:32, 128 * p : 128 * p + 128]
    bottom = y[32:64, 128 * p : 128 * p + 128]
    first = jnp.where(lane < 64, top, pltpu.roll(bottom, 64, 1))
    second = jnp.where(lane < 64, pltpu.roll(top, 64, 1), bottom)
    return first.astype(BF16), second.astype(BF16)


def unpacked(first, second):
    lane = lax.broadcasted_iota(jnp.int32, (32, 128), 1)
    a, b = first.astype(F32), second.astype(F32)
    top = jnp.where(lane < 64, a, pltpu.roll(b, 64, 1))
    bottom = jnp.where(lane < 64, pltpu.roll(a, 64, 1), b)
    return top.astype(BF16), bottom.astype(BF16)


def kernel(
    tok, route, rw, gain, gw, uw, dw,
    mixed, gate_o, up_o, down_o,
    wst, gus, dns, gu, dn, dn2, disp, arr, xg, ssq, hid, part, s_r, s_l, r_r, r_l, yv, back, ret, hits,
    load_sem, out_sem,
    ts_sem, tr_sem, gs_sem, gr_sem, ds_sem, dr_sem, bs_sem, br_sem,
    agrs, agrr, agls, aglr, pas, par, exs, exr, rrs, rrr, rls, rlr,
):
    fs = lax.axis_index("fs")
    tp = lax.axis_index("tp")
    z = tp // 2
    c = tp % 2
    partner = (fs, tp + 1 - 2 * c)
    right = (fs, ((z + 1) % NZ) * 2 + c)
    left = (fs, ((z + NZ - 1) % NZ) * 2 + c)

    def rcopy(src, dst, ss, rs, dev):
        return pltpu.make_async_remote_copy(
            src_ref=src, dst_ref=dst, send_sem=ss, recv_sem=rs, device_id=dev, device_id_type=MESH
        )

    def peer(k):
        return (fs + k) % FS

    loads = [
        pltpu.make_async_copy(w, wst.at[i], load_sem.at[i]) for i, w in enumerate((gw, uw, dw))
    ]
    for ld in loads:
        ld.start()

    barrier = pltpu.get_barrier_semaphore()

    @pl.loop(1, FS)
    def _(k):
        pl.semaphore_signal(barrier, inc=1, device_id=(peer(k), tp), device_id_type=MESH)

    for dev in (partner, right, left):
        pl.semaphore_signal(barrier, inc=1, device_id=dev, device_id_type=MESH)

    r0, r1 = route[0:1, :], route[1:2, :]
    ex = lax.broadcasted_iota(jnp.int32, (16, 256), 0)
    m0, m1 = ex == r0, ex == r1
    named = jnp.where(m0 | m1, 1.0, 0.0).astype(BF16)
    earlier = jnp.where(
        lax.broadcasted_iota(jnp.int32, (256, 256), 0) < lax.broadcasted_iota(jnp.int32, (256, 256), 1), 1.0, 0.0
    ).astype(BF16)
    before = jnp.dot(named, earlier, preferred_element_type=F32)
    t0 = r0 * 64 + jnp.sum(jnp.where(m0, before, 0.0), axis=0, keepdims=True).astype(jnp.int32)
    t1 = r1 * 64 + jnp.sum(jnp.where(m1, before, 0.0), axis=0, keepdims=True).astype(jnp.int32)
    row = lax.broadcasted_iota(jnp.int32, (1024, 256), 0)
    hits[0] = jnp.where(row == t0, 1.0, 0.0).astype(BF16)
    hits[1] = jnp.where(row == t1, 1.0, 0.0).astype(BF16)
    d = lax.dot_general(
        tok[...], hits[0] + hits[1], (((1,), (1,)), ((), ())), preferred_element_type=F32
    )
    for p in range(8):
        a, b = packed(d, p)
        disp[2 * p] = a
        disp[2 * p + 1] = b

    pl.semaphore_wait(barrier, FS - 1 + 3)

    def tok_copy(to, src):
        return rcopy(disp.at[to], arr.at[src], ts_sem.at[to], tr_sem.at[src], (to, tp))

    @pl.loop(1, FS)
    def _(k):
        tok_copy(peer(k), fs).start()

    arr[fs] = disp[fs]

    eye = lax.broadcasted_iota(jnp.int32, (128, 128), 0) == lax.broadcasted_iota(jnp.int32, (128, 128), 1)
    gcol = jnp.sum(jnp.where(eye, gain[...], 0.0), axis=1, keepdims=True)
    loads[0].wait()
    loads[1].wait()

    @pl.loop(0, FS)
    def _(e):
        gus[e, :, 0:128] = (wst[0, e] * gcol).astype(BF16)
        gus[e, :, 128:256] = (wst[1, e] * gcol).astype(BF16)

    def gu_copy(to, src):
        return rcopy(gus.at[to], gu.at[src], gs_sem.at[to], gr_sem.at[src], (to, tp))

    def dn_copy(to, src):
        return rcopy(dns.at[to], dn.at[src], ds_sem.at[to], dr_sem.at[src], (to, tp))

    @pl.loop(1, FS)
    def _(k):
        gu_copy(peer(k), fs).start()

    gu[fs] = gus[fs]
    loads[2].wait()

    @pl.loop(0, FS)
    def _(e):
        dns[e] = wst[2, e].astype(BF16)

    @pl.loop(1, FS)
    def _(k):
        dn_copy(peer(k), fs).start()

    dn[fs] = dns[fs]

    @pl.loop(1, FS)
    def _(k):
        tok_copy(fs, peer(k)).wait_recv()

    for p in range(8):
        top, bottom = unpacked(arr[2 * p], arr[2 * p + 1])
        xg[tp, 0:32, 128 * p : 128 * p + 128] = top
        xg[tp, 32:64, 128 * p : 128 * p + 128] = bottom

    def ag(block, s, q, ss, rs, dev):
        piece = xg.at[block, pl.ds(16 * q, 16)]
        return rcopy(piece, piece, ss.at[s, q], rs.at[s, q], dev)

    def ag_r(s, q):
        return ag(((z + NZ - s) % NZ) * 2 + c, s, q, agrs, agrr, right)

    def ag_l(s, q):
        return ag(((z + s) % NZ) * 2 + c, s, q, agls, aglr, left)

    def ag_rw(s, q):
        return ag(((z + NZ - 1 - s) % NZ) * 2 + c, s, q, agrs, agrr, right)

    def ag_lw(s, q):
        return ag(((z + 1 + s) % NZ) * 2 + c, s, q, agls, aglr, left)

    def shared(block, n):
        return rcopy(xg.at[block], xg.at[block], pas.at[n], par.at[n], partner)

    for q in range(QUARTERS):
        ag_r(0, q).start()
        ag_l(0, q).start()
    shared(tp, 0).start()

    def squares(block):
        v = xg[block].astype(F32)
        v = v * v
        t = v[0:8]
        for i in range(1, 8):
            t = t + v[8 * i : 8 * i + 8]
        return t

    ssq[...] = squares(tp)

    def ag_step(s, last):
        for q in range(QUARTERS):
            ag_rw(s, q).wait_recv()
            if not last or q < 2:
                ag_r(s + 1, q).start()
            ag_lw(s, q).wait_recv()
            if not last or q >= 2:
                ag_l(s + 1, q).start()
        br = ((z + NZ - 1 - s) % NZ) * 2 + c
        bl = ((z + 1 + s) % NZ) * 2 + c
        shared(br, 1 + 2 * s).start()
        shared(bl, 2 + 2 * s).start()
        ssq[...] += squares(br) + squares(bl)

    @pl.loop(0, HALF - 2)
    def _(s):
        ag_step(s, False)

    ag_step(HALF - 2, True)
    for q in range(2):
        ag_rw(HALF - 1, q).wait_recv()
        ag_lw(HALF - 1, q + 2).wait_recv()
    far = ((z + HALF) % NZ) * 2 + c
    shared(far, NZ - 1).start()
    ssq[...] += squares(far)

    @pl.loop(1, FS)
    def _(k):
        gu_copy(fs, peer(k)).wait_recv()

    @pl.loop(1, FS)
    def _(k):
        dn_copy(fs, peer(k)).wait_recv()

    outs = [
        pltpu.make_async_copy(gu.at[:, :, 0:128], gate_o, out_sem.at[0]),
        pltpu.make_async_copy(gu.at[:, :, 128:256], up_o, out_sem.at[1]),
        pltpu.make_async_copy(dn, down_o, out_sem.at[2]),
    ]
    for o in outs:
        o.start()
    own_half = pl.multiple_of(c * 64, 64)
    other_half = pl.multiple_of(64 - c * 64, 64)
    dn_swap = rcopy(
        dn.at[:, pl.ds(other_half, 64), :], dn2.at[:, :, 128:256], exs.at[0], exr.at[0], partner
    )
    dn_swap.start()
    dn2[:, :, 0:128] = dn[:, pl.ds(own_half, 64), :]

    other = 1 - 2 * c

    @pl.loop(0, NZ)
    def _(n):
        shared(tp + other, n).wait_recv()

    @pl.loop(0, NZ)
    def _(n):
        ssq[...] += squares(2 * n + 1 - c)

    total = jnp.sum(ssq[...], axis=0, keepdims=True)
    scale = lax.rsqrt(total / 2048.0 + EPS)
    acc = lax.dot_general(
        gu[...].reshape(2048, 256),
        xg[...].reshape(2048, 1024),
        (((0,), (0,)), ((), ())),
        preferred_element_type=F32,
    )
    g = acc[0:128] * scale
    u = acc[128:256] * scale
    hid[0:128] = (g / (1.0 + jnp.exp(-g)) * u).astype(BF16)
    hid_swap = rcopy(hid.at[0:128], hid.at[128:256], exs.at[1], exr.at[1], partner)
    hid_swap.start()
    dn_swap.wait_recv()
    hid_swap.wait_recv()

    def rs_r(s, q):
        rows = pl.ds(16 * q, 16)
        return rcopy(s_r.at[s, rows], r_r.at[s, rows], rrs.at[s, q], rrr.at[s, q], right)

    def rs_l(s, q):
        rows = pl.ds(16 * q, 16)
        return rcopy(s_l.at[s, rows], r_l.at[s, rows], rls.at[s, q], rlr.at[s, q], left)

    fa = jnp.dot(dn2[(z + HALF) % NZ], hid[...], preferred_element_type=F32).astype(BF16)
    s_r[0, 0:32] = fa[0:32]
    s_l[0, 32:64] = fa[32:64]
    for q in range(2):
        rs_r(0, q).start()
        rs_l(0, q + 2).start()
    part[...] = jnp.dot(
        dn2[...].reshape(1024, 256), hid[...], preferred_element_type=F32
    ).reshape(16, 64, 1024)

    def rs_step(s, first):
        dr = (z + HALF - s) % NZ
        dl = (z + HALF + s) % NZ
        for q in range(QUARTERS):
            rows = pl.ds(16 * q, 16)
            v = part[dr, rows]
            if not first or q < 2:
                rs_r(s - 1, q).wait_recv()
                v = v + r_r[s - 1, rows].astype(F32)
            s_r[s, rows] = v.astype(BF16)
            rs_r(s, q).start()
            v = part[dl, rows]
            if not first or q >= 2:
                rs_l(s - 1, q).wait_recv()
                v = v + r_l[s - 1, rows].astype(F32)
            s_l[s, rows] = v.astype(BF16)
            rs_l(s, q).start()

    rs_step(1, True)

    @pl.loop(2, HALF)
    def _(s):
        rs_step(s, False)

    for q in range(QUARTERS):
        rows = pl.ds(16 * q, 16)
        rs_r(HALF - 1, q).wait_recv()
        rs_l(HALF - 1, q).wait_recv()
        yv[rows] = (
            part[z, rows] + r_r[HALF - 1, rows].astype(F32) + r_l[HALF - 1, rows].astype(F32)
        )

    for p in range(8):
        a, b = packed(yv[...], p)
        back[2 * p] = a
        back[2 * p + 1] = b

    def back_copy(to, src):
        return rcopy(back.at[to], ret.at[src], bs_sem.at[to], br_sem.at[src], (to, tp))

    @pl.loop(1, FS)
    def _(k):
        back_copy(peer(k), fs).start()

    ret[fs] = back[fs]

    @pl.loop(1, FS)
    def _(k):
        tok_copy(peer(k), fs).wait_send()
        gu_copy(peer(k), fs).wait_send()
        dn_copy(peer(k), fs).wait_send()

    @pl.loop(0, NZ)
    def _(n):
        shared(tp, n).wait_send()

    @pl.loop(0, HALF - 1)
    def _(s):
        for q in range(QUARTERS):
            ag_r(s, q).wait_send()
            ag_l(s, q).wait_send()
            rs_r(s + 1, q).wait_send()
            rs_l(s + 1, q).wait_send()

    for q in range(2):
        ag_r(HALF - 1, q).wait_send()
        ag_l(HALF - 1, q + 2).wait_send()
        rs_r(0, q).wait_send()
        rs_l(0, q + 2).wait_send()
    dn_swap.wait_send()
    hid_swap.wait_send()
    for o in outs:
        o.wait()

    @pl.loop(1, FS)
    def _(k):
        back_copy(fs, peer(k)).wait_recv()

    tops, bottoms = [], []
    for p in range(8):
        top, bottom = unpacked(ret[2 * p], ret[2 * p + 1])
        tops.append(top)
        bottoms.append(bottom)
    got = jnp.concatenate(
        [jnp.concatenate(tops, axis=1), jnp.concatenate(bottoms, axis=1)], axis=0
    )
    first = jnp.dot(got, hits[0], preferred_element_type=F32)
    second = jnp.dot(got, hits[1], preferred_element_type=F32)
    mixed[...] = (first * rw[0:1, :] + second * rw[1:2, :]).astype(BF16)

    @pl.loop(1, FS)
    def _(k):
        back_copy(peer(k), fs).wait_send()


def body(tokens, norm_gain, gate_weight, up_weight, down_weight, route, route_weight):
    vm = pl.BlockSpec(memory_space=pltpu.VMEM)
    anywhere = pl.BlockSpec(memory_space=pl.ANY)
    dma = pltpu.SemaphoreType.DMA
    weight = jax.ShapeDtypeStruct((16, 128, 128), BF16)
    mixed, g, u, d = pl.pallas_call(
        kernel,
        out_shape=(jax.ShapeDtypeStruct((64, 256), BF16), weight, weight, weight),
        in_specs=[vm, vm, vm, vm, anywhere, anywhere, anywhere],
        out_specs=(vm, anywhere, anywhere, anywhere),
        scratch_shapes=[
            pltpu.VMEM((3, 16, 128, 128), F32),
            pltpu.VMEM((16, 128, 256), BF16),
            pltpu.VMEM((16, 128, 128), BF16),
            pltpu.VMEM((16, 128, 256), BF16),
            pltpu.VMEM((16, 128, 128), BF16),
            pltpu.VMEM((16, 64, 256), BF16),
            pltpu.VMEM((16, 32, 128), BF16),
            pltpu.VMEM((16, 32, 128), BF16),
            pltpu.VMEM((32, 64, 1024), BF16),
            pltpu.VMEM((8, 1024), F32),
            pltpu.VMEM((256, 1024), BF16),
            pltpu.VMEM((16, 64, 1024), F32),
            pltpu.VMEM((8, 64, 1024), BF16),
            pltpu.VMEM((8, 64, 1024), BF16),
            pltpu.VMEM((8, 64, 1024), BF16),
            pltpu.VMEM((8, 64, 1024), BF16),
            pltpu.VMEM((64, 1024), F32),
            pltpu.VMEM((16, 32, 128), BF16),
            pltpu.VMEM((16, 32, 128), BF16),
            pltpu.VMEM((2, 1024, 256), BF16),
            dma((3,)),
            dma((3,)),
            dma((16,)), dma((16,)),
            dma((16,)), dma((16,)),
            dma((16,)), dma((16,)),
            dma((16,)), dma((16,)),
            dma((8, 4)), dma((8, 4)),
            dma((8, 4)), dma((8, 4)),
            dma((16,)), dma((16,)),
            dma((2,)), dma((2,)),
            dma((8, 4)), dma((8, 4)),
            dma((8, 4)), dma((8, 4)),
        ],
        compiler_params=pltpu.CompilerParams(
            collective_id=0, has_side_effects=True, vmem_limit_bytes=50 * 1024 * 1024
        ),
        name="moe",
    )(
        tokens.T,
        route.T,
        route_weight.T,
        norm_gain.reshape(1, 128),
        gate_weight,
        up_weight,
        down_weight,
    )
    out = (1, 2048, 128)
    return mixed.T, g.reshape(out), u.reshape(out), d.reshape(out)


def solution(mesh):
    in_specs = (
        P("fs", "tp"),
        P("fs"),
        P(None, "fs", "tp"),
        P(None, "fs", "tp"),
        P(None, "fs", "tp"),
        P("fs", None),
        P("fs", None),
    )
    out_specs = (P("fs", "tp"), P("fs", None, "tp"), P("fs", None, "tp"), P("fs", None, "tp"))
    return jax.shard_map(body, mesh=mesh, in_specs=in_specs, out_specs=out_specs, check_vma=False)
```

time: 260 us -> 105 us (0.40)
  the two profiles are of different devices: /device:TPU:32 before, /device:TPU:4 now
where the time goes in v1:
time: 105 us; the launch traced here: 104 us
  Pallas kernels  96.8 us (92%)
  local copies, waits for them, and re-layouts  6.88 us (7%)
    pallas_call x1, Pallas kernels, body(): pl.pallas_call(kernel, out_shape=(jax.ShapeDtypeStruct((64, 256), BF16),...  96.8 us
    unnamed x16, local copies, waits for them, and re-layouts  6.88 us

profile of v1, /device:TPU:4, one launch (start us, length us, event | category | flops | bytes accessed | tf_op | source)
XLA Modules:
  0.0 104.4 jit_solution(2843932615990805175)
XLA Ops:
  0.6 0.0 copy-start.4
  0.6 0.0 copy-start.3
  0.7 0.0 copy-start.5
  0.7 0.7 copy-done.4
  1.3 0.0 copy-done.3
  1.3 0.0 copy-done.5
  1.3 0.0 copy-start
  1.3 1.2 %copy-done = f32[16,128,128]{2,1,0:T(8,128)S(1)} copy-done((f32[16,128,128]{2,1,0:T(8,128)S(1)}, f32[16,128,128]{2,1,0:T(8,128)}, u32[]{:S(2)}) %copy-start) | copy-done | bytes 1048600
  2.6 0.0 copy-start.1
  2.6 1.2 %copy-done.1 = f32[16,128,128]{2,1,0:T(8,128)S(1)} copy-done((f32[16,128,128]{2,1,0:T(8,128)S(1)}, f32[16,128,128]{2,1,0:T(8,128)}, u32[]{:S(2)}) %copy-start.1) | copy-done | bytes 1048600
  3.8 0.0 copy-start.2
  3.8 0.8 copy-done.2
  4.5 96.8 %moe.1 = (bf16[64,256]{1,0:T(8,128)(2,1)S(1)}, bf16[16,128,128]{2,1,0:T(8,128)(2,1)S(1)}, bf16[16,128,128]{2,1,0:T(8,128)(2,1)S(1)}, bf16[16,128,128]{2,1,0:T(8,128)(2,1)S(1)}) custom-call(bf16[64,256]{1,0:T(8,128)(2,1)S(1)} %bitcast.11, s32[2,256]{1,0:T(2,128)S(1)} %bitcast.13, f32[2,256]{1,0:T(2,128)S(1)} %bitcast.14, f32[1,128]{1,0:T(1,128)S(1)} %bitcast.15, ...), custom_call_target="tpu_custom_call" | custom-call | tf_op jit(solution)/shard_map/moe/pallas_call | solution.py:376
  101.4 0.6 copy.15
  102.0 0.8 copy.16
  102.8 0.8 copy.17
  103.6 0.8 copy.18
Async XLA Ops:
  0.6 0.7 copy-start.4
  0.6 0.7 copy-start.3
  0.7 0.7 copy-start.5
  1.3 1.2 %copy-start = (f32[16,128,128]{2,1,0:T(8,128)S(1)}, f32[16,128,128]{2,1,0:T(8,128)}, u32[]{:S(2)}) copy-start(f32[16,128,128]{2,1,0:T(8,128)} %gw.1) | copy-start | bytes 3145732
  2.6 1.2 %copy-start.1 = (f32[16,128,128]{2,1,0:T(8,128)S(1)}, f32[16,128,128]{2,1,0:T(8,128)}, u32[]{:S(2)}) copy-start(f32[16,128,128]{2,1,0:T(8,128)} %uw.1) | copy-start | bytes 3145732
  3.8 0.8 copy-start.2
